TPU v7x, 32 devices: a whole 2x2x4 slice. The times are simulated.
32 devices in a mesh: sp: 8 (over z, x), tp: 4 (over y, core).
Axes of the slice: x: 2, y: 2, z: 4, core: 2. Of those that a mesh axis runs over, the one named last changes fastest.
Arguments:
- residual: bfloat16 [2048, 2048], P(('sp', 'tp')), may hold values from -6 to 6
- queries: bfloat16 [2048, 1024], P('sp', 'tp'), may hold values from -8 to 8
- key_pairs: bfloat16 [2048, 512], P('sp', 'tp'), may hold values from -8 to 8
- values: bfloat16 [2048, 512], P('sp', 'tp'), may hold values from -6 to 6
- lambdas: float32 [8], P('tp'), may hold values from 0.3 to 0.8
- head_gain: float32 [128], replicated, may hold values from 0.1 to 1.9
- out_weight: bfloat16 [1024, 2048], replicated, may hold values from -0.1875 to 0.1875
- mixer_gain: float32 [2048], replicated, may hold values from 0.1 to 1.9
- before_gain: float32 [2048], replicated, may hold values from 0.1 to 1.9
- after_gain: float32 [2048], replicated, may hold values from 0.1 to 1.9
- gate_weight: bfloat16 [2048, 5632], P('sp', 'tp'), may hold values from -0.125 to 0.125
- up_weight: bfloat16 [2048, 5632], P('sp', 'tp'), may hold values from -0.125 to 0.125
- down_weight: bfloat16 [5632, 2048], P('tp', 'sp'), may hold values from -0.078125 to 0.078125
Outputs:
- updated: bfloat16 [2048, 2048], P(('sp', 'tp'))
All inputs are finite; a program needn't handle non-finite values.
Results may differ from a plain program's by a relative error of at most 0.014.
Values may be sent and summed in bfloat16 or wider, within the bound.
A program may use at most 128 MiB of HBM per device.

v0:
```python
import math
import jax
import jax.numpy as jnp
from jax import lax
from jax.sharding import PartitionSpec as P

HEAD_DIM = 64


def row_norm(values_in, gain, epsilon):
    mean_square = jnp.mean(values_in * values_in, axis=-1, keepdims=True)
    return values_in * lax.rsqrt(mean_square + epsilon) * gain


def on_device(
    residual,
    queries,
    key_pairs,
    values,
    lambdas,
    head_gain,
    out_weight,
    mixer_gain,
    before_gain,
    after_gain,
    gate_weight,
    up_weight,
    down_weight,
):
    tokens_here = queries.shape[0]
    quarter = residual.shape[0]
    width = 2 * HEAD_DIM
    local_heads = queries.shape[1] // width
    scale = 1.0 / math.sqrt(HEAD_DIM)
    height = local_heads * tokens_here
    query_rows = jnp.transpose(
        queries.reshape(tokens_here, local_heads, 2, HEAD_DIM), (2, 1, 0, 3)
    ).reshape(2, height, HEAD_DIM)
    empty = (
        jnp.full((height,), -1e30, jnp.float32),
        jnp.zeros((height,), jnp.float32),
        jnp.zeros((height, width), jnp.float32),
    )
    state = (empty, empty)
    key_piece = lax.all_gather(key_pairs, "sp", axis=0, tiled=True)
    value_piece = lax.all_gather(values, "sp", axis=0, tiled=True)
    length = key_piece.shape[0]
    span = length
    for split_count in range(1, length + 1):
        if length % split_count == 0 and length // split_count <= 2048:
            span = length // split_count
            break
    key_blocks = key_piece.reshape(length // span, span, 2, HEAD_DIM)
    value_blocks = value_piece.reshape(length // span, span, width)

    def advance(carry, blocks_in):
        key_block, value_block = blocks_in
        renewed = []
        for which in range(2):
            running_top, running_total, running_numer = carry[which]
            score = (
                jnp.dot(
                    query_rows[which], key_block[:, which].T, preferred_element_type=jnp.float32
                )
                * scale
            )
            new_top = jnp.maximum(running_top, jnp.max(score, axis=1))
            shrink = jnp.exp(running_top - new_top)
            expo = jnp.exp(score - new_top[:, None])
            new_total = running_total * shrink + jnp.sum(expo, axis=1)
            new_numer = running_numer * shrink[:, None] + jnp.dot(
                expo.astype(jnp.bfloat16), value_block, preferred_element_type=jnp.float32
            )
            renewed.append((new_top, new_total, new_numer))
        return (tuple(renewed), None)

    state, _ = lax.scan(advance, state, (key_blocks, value_blocks))
    first_map, second_map = state
    lambda_rows = jnp.repeat(lambdas, tokens_here)[:, None]
    attended = first_map[2] / first_map[1][:, None] - lambda_rows * (
        second_map[2] / second_map[1][:, None]
    )
    normed = row_norm(attended, head_gain, 1e-05).astype(jnp.bfloat16)
    head_out = jnp.transpose(normed.reshape(local_heads, tokens_here, width), (1, 0, 2)).reshape(
        tokens_here, local_heads * width
    )
    grouped = head_out.reshape(lax.axis_size("tp"), quarter, local_heads * width)
    mixed = jnp.dot(
        lax.all_to_all(grouped, "tp", split_axis=0, concat_axis=2, tiled=True)[0],
        out_weight,
        preferred_element_type=jnp.float32,
    ).astype(jnp.bfloat16)[None][0]
    stream = residual.astype(jnp.float32) + row_norm(mixed.astype(jnp.float32), mixer_gain, 1e-06)
    normed_in = row_norm(stream, before_gain, 1e-06).astype(jnp.bfloat16)
    gathered = lax.all_gather(normed_in, "tp", axis=0, tiled=True)
    empty_hidden = jnp.zeros((gathered.shape[0], gate_weight.shape[1]), jnp.float32)
    pieces = (
        lax.all_gather(gate_weight, "sp", axis=0, tiled=True),
        lax.all_gather(up_weight, "sp", axis=0, tiled=True),
    )
    columns = lax.slice_in_dim(gathered, 0, pieces[0].shape[0], axis=1)
    gate_part = jnp.dot(columns, pieces[0], preferred_element_type=jnp.float32)
    up_part = jnp.dot(columns, pieces[1], preferred_element_type=jnp.float32)
    gate = empty_hidden + gate_part
    up = empty_hidden + up_part
    down_whole = lax.all_gather(down_weight, "sp", axis=1, tiled=True)
    hidden = (jax.nn.silu(gate) * up).astype(jnp.bfloat16)
    picked = lax.slice_in_dim(hidden, 0, lax.axis_size("tp") * quarter, axis=0)
    channel = lax.psum_scatter(
        jnp.dot(picked, down_whole, preferred_element_type=jnp.float32).astype(jnp.bfloat16),
        "tp",
        scatter_dimension=0,
        tiled=True,
    )
    updated = stream + 0.5 * row_norm(channel.astype(jnp.float32), after_gain, 1e-06)
    return updated.astype(jnp.bfloat16)


def solution(mesh):
    return jax.shard_map(
        on_device,
        mesh=mesh,
        in_specs=(
            P(("sp", "tp"), None),
            P("sp", "tp"),
            P("sp", "tp"),
            P("sp", "tp"),
            P("tp"),
            P(),
            P(),
            P(),
            P(),
            P(),
            P("sp", "tp"),
            P("sp", "tp"),
            P("tp", "sp"),
        ),
        out_specs=P(("sp", "tp"), None),
        check_vma=False,
    )
```

profile of v0, /device:TPU:0, one launch (start us, length us, event | category | flops | bytes accessed | tf_op | source)
XLA Modules:
  0.0 430.2 jit_solution(3633528644462433819)
XLA Ops:
  6.5 0.0 copy-start
  6.5 0.0 all-gather.5.cloned.1.call-start
  6.5 0.9 copy.16
  7.5 33.0 %all_gather.18 = bf16[2048,128]{0,1:T(8,128)(2,1)S(1)} all-gather(bf16[256,128]{0,1:T(8,128)(2,1)S(1)} %copy.16), channel_id=1, replica_groups=mesh['sp'=8,'tp'=4] {'sp'}, dimensions={0}, use_global_device_ids=true | all-gather | bytes 589824 | tf_op jit(solution)/shard_map/all_gather | solution.py:45
  40.5 1.0 copy.14
  41.6 0.1 copy.15
  41.7 0.0 copy-start.3
  41.7 0.8 multiply_reduce_fusion.1
  42.5 0.8 fusion
  43.3 0.0 copy-done.3
  43.3 31.3 %all_gather.19 = bf16[2048,128]{1,0:T(8,128)(2,1)S(1)} all-gather(bf16[256,128]{1,0:T(8,128)(2,1)S(1)} %copy-done.3), channel_id=1, replica_groups=mesh['sp'=8,'tp'=4] {'sp'}, dimensions={0}, use_global_device_ids=true | all-gather | bytes 589824 | tf_op jit(solution)/shard_map/all_gather | solution.py:46
  74.6 0.1 copy.17
  74.7 0.8 multiply_reduce_fusion
  75.5 0.8 fusion.2
  76.4 0.0 copy-done
  76.4 0.1 broadcast_bitcast_fusion
  76.5 0.9 fusion.29
  77.3 0.0 copy-start.6
  77.4 1.5 multiply_reduce_fusion.4
  78.8 0.0 copy-start.1
  78.9 0.0 copy-start.2
  78.9 0.0 copy-start.4
  78.9 0.0 copy-done.6
  78.9 0.1 multiply_convert_fusion.1
  79.0 0.1 copy.25
  79.2 0.1 reshape_reshape.3
  79.3 7.2 %all_to_all.15 = bf16[4,64,256]{2,1,0:T(8,128)(2,1)S(1)} all-to-all(bf16[4,64,256]{2,1,0:T(8,128)(2,1)S(1)} %reshape_reshape.3), channel_id=1, replica_groups=mesh['sp'=8,'tp'=4] {'tp'}, dimensions={0} | all-to-all | bytes 262144 | tf_op jit(solution)/shard_map/all_to_all | solution.py:89
  86.5 0.1 copy.19
  86.6 3.1 multiply_reduce_fusion.3
  89.8 0.0 copy-done.1
  89.8 0.0 copy-done.2
  89.8 0.3 multiply_reduce_fusion.2
  90.1 0.0 copy-done.4
  90.1 0.9 multiply_convert_fusion
  91.0 0.0 all-gather.5.cloned.1.call-update
  91.0 0.0 all-gather.7.cloned.1.call-start
  91.0 0.7 all-gather.7.cloned.1.call-update
  91.8 0.0 all-gather.11.cloned.1.call-start
  91.8 0.7 all-gather.11.cloned.1.call-update
  92.5 0.0 all-gather.9.cloned.1.call-start
  92.5 0.5 all-gather.9.cloned.1.call-update
  93.1 0.0 reduce-scatter.2.cloned.1.call-start
  93.1 15.0 %all-gather.5.cloned.1.call-done = bf16[256,2048]{1,0:T(8,128)(2,1)} async-done(((bf16[64,2048]{1,0:T(8,128)(2,1)}), bf16[256,2048]{1,0:T(8,128)(2,1)}) %all-gather.5.cloned.1.call-update) | async-done | bytes 1048592 | tf_op jit(solution)/shard_map/all_gather | solution.py:95
  108.1 0.0 copy-start.7
  108.1 94.5 %all-gather.7.cloned.1.call-done = bf16[2048,1408]{1,0:T(8,128)(2,1)} async-done(((bf16[256,1408]{1,0:T(8,128)(2,1)}), bf16[2048,1408]{1,0:T(8,128)(2,1)}) %all-gather.7.cloned.1.call-update) | async-done | bytes 5767184 | tf_op jit(solution)/shard_map/all_gather | solution.py:98
  202.6 4.8 %fusion.45 = f32[256,1408]{1,0:T(8,128)S(1)} fusion(bf16[256,2048]{1,0:T(8,128)(2,1)} %all-gather.5.cloned.1.call-done, bf16[2048,1408]{1,0:T(8,128)(2,1)} %all-gather.7.cloned.1.call-done), kind=kOutput, calls=%fused_computation.58 | convolution fusion | flops 1476395008 | bytes 8257536 | tf_op jit(solution)/shard_map/dot_general | solution.py:102
  207.4 0.0 copy-start.5
  207.4 88.6 %all-gather.11.cloned.1.call-done = bf16[1408,2048]{1,0:T(8,128)(2,1)} async-done(((bf16[1408,256]{1,0:T(8,128)(2,1)}), bf16[1408,2048]{1,0:T(8,128)(2,1)}) %all-gather.11.cloned.1.call-update) | async-done | bytes 5767184 | tf_op jit(solution)/shard_map/all_gather | solution.py:106
  296.0 92.6 %all-gather.9.cloned.1.call-done = bf16[2048,1408]{1,0:T(8,128)(2,1)} async-done(((bf16[256,1408]{1,0:T(8,128)(2,1)}), bf16[2048,1408]{1,0:T(8,128)(2,1)}) %all-gather.9.cloned.1.call-update) | async-done | bytes 5767184 | tf_op jit(solution)/shard_map/all_gather | solution.py:99
  388.6 0.0 copy-done.7
  388.6 8.9 %convolution_convert_fusion = bf16[256,2048]{1,0:T(8,128)(2,1)} fusion(bf16[1408,2048]{1,0:T(8,128)(2,1)} %all-gather.11.cloned.1.call-done, bf16[256,2048]{1,0:T(8,128)(2,1)S(1)} %copy-done.7, bf16[2048,1408]{1,0:T(8,128)(2,1)} %all-gather.9.cloned.1.call-done, f32[256,1408]{1,0:T(8,128)S(1)} %fusion.45), kind=kOutput, calls=%fused_computation.10 | convolution fusion | flops 2955476992 | bytes 15073280 | tf_op jit(solution)/shard_map/dot_general | solution.py:110
  397.5 0.0 reduce-scatter.2.cloned.1.call-update
  397.5 23.1 %reduce-scatter.2.cloned.1.call-done = bf16[64,2048]{1,0:T(8,128)(2,1)} async-done(((bf16[256,2048]{1,0:T(8,128)(2,1)}), bf16[64,2048]{1,0:T(8,128)(2,1)}) %reduce-scatter.2.cloned.1.call-update) | async-done | bytes 262160 | tf_op jit(solution)/shard_map/reduce_scatter | solution.py:109
  420.6 1.1 fusion.32
  421.7 0.0 copy-done.5
  421.7 1.9 fusion.36
  (13 shorter events, 0.1 us)
Async XLA Ops:
  6.5 69.8 %copy-start = (f32[2]{0:T(128)S(1)}, f32[2]{0:T(128)}, u32[]{:S(2)}) copy-start(f32[2]{0:T(128)} %param.17) | copy-start | bytes 28
  6.5 101.6 %all-gather.5.cloned.1.call-start = ((), (), s32[]{:S(2)}) async-start(), calls=%async_computation.2 | async-start | bytes 1310720 | tf_op jit(solution)/shard_map/all_gather | solution.py:95
  41.7 1.7 copy-start.3
  77.3 1.6 copy-start.6
  78.8 10.9 %copy-start.1 = (bf16[64,2048]{1,0:T(8,128)(2,1)S(1)}, bf16[64,2048]{1,0:T(8,128)(2,1)}, u32[]{:S(2)}) copy-start(bf16[64,2048]{1,0:T(8,128)(2,1)} %param.13) | copy-start | bytes 786436
  78.9 10.9 %copy-start.2 = (f32[2048]{0:T(1024)S(1)}, f32[2048]{0:T(1024)}, u32[]{:S(2)}) copy-start(f32[2048]{0:T(1024)} %param.20) | copy-start | bytes 24580
  78.9 11.2 %copy-start.4 = (f32[2048]{0:T(1024)S(1)}, f32[2048]{0:T(1024)}, u32[]{:S(2)}) copy-start(f32[2048]{0:T(1024)} %param.21) | copy-start | bytes 24580
  91.0 111.6 %all-gather.7.cloned.1.call-start = ((), (), s32[]{:S(2)}) async-start(), calls=%async_computation.3 | async-start | bytes 6488064 | tf_op jit(solution)/shard_map/all_gather | solution.py:98
  91.8 204.3 %all-gather.11.cloned.1.call-start = ((), (), s32[]{:S(2)}) async-start(), calls=%async_computation.5 | async-start | bytes 6488064 | tf_op jit(solution)/shard_map/all_gather | solution.py:106
  92.5 296.1 %all-gather.9.cloned.1.call-start = ((), (), s32[]{:S(2)}) async-start(), calls=%async_computation.4 | async-start | bytes 6488064 | tf_op jit(solution)/shard_map/all_gather | solution.py:99
  93.1 327.5 %reduce-scatter.2.cloned.1.call-start = ((), (), s32[]{:S(2)}) async-start(), calls=%async_computation.6 | async-start | bytes 1310720 | tf_op jit(solution)/shard_map/reduce_scatter | solution.py:109
  108.1 280.5 %copy-start.7 = (bf16[256,2048]{1,0:T(8,128)(2,1)S(1)}, bf16[256,2048]{1,0:T(8,128)(2,1)}, u32[]{:S(2)}) copy-start(bf16[256,2048]{1,0:T(8,128)(2,1)} %all-gather.5.cloned.1.call-done) | copy-start | bytes 3145732
  207.4 214.3 %copy-start.5 = (f32[2048]{0:T(1024)S(1)}, f32[2048]{0:T(1024)}, u32[]{:S(2)}) copy-start(f32[2048]{0:T(1024)} %param.22) | copy-start | bytes 24580
Sparse Core Ops, SparseCore 0:
  91.1 16.9 all-gather.4
  110.3 92.2 all-gather.6
  204.7 91.2 all-gather.10
  298.1 90.4 all-gather.8
  397.6 22.9 reduce-scatter.1
where the time goes:
time: 431 us; the launch traced here: 430 us
  waiting for transfers between devices  316 us (73%)
  blocking collectives  71.5 us (17%)
  matrix products  20.8 us (5%)
  between operations  13.4 us (3%)
  other arithmetic  6.02 us (1%)
    all_gather x1, waiting for transfers between devices, on_device(): lax.all_gather(gate_weight, 'sp', axis=0, tiled=True)  94.5 us
    all_gather x1, waiting for transfers between devices, on_device(): lax.all_gather(up_weight, 'sp', axis=0, tiled=True)  92.6 us
    all_gather x1, waiting for transfers between devices, on_device(): down_whole = lax.all_gather(down_weight, 'sp', axis=1, tiled=True)  88.6 us
    all_gather x1, blocking collectives, on_device(): key_piece = lax.all_gather(key_pairs, 'sp', axis=0, tiled=True)  33 us
    all_gather x1, blocking collectives, on_device(): value_piece = lax.all_gather(values, 'sp', axis=0, tiled=True)  31.3 us
    reduce_scatter x1, waiting for transfers between devices, on_device(): lax.psum_scatter(jnp.dot(picked, down_whole, preferred_element_type=jnp.f...  23.1 us
    all_gather x1, waiting for transfers between devices, on_device(): gathered = lax.all_gather(normed_in, 'tp', axis=0, tiled=True)  15 us
    dot_general x1, matrix products, on_device(): jnp.dot(picked, down_whole, preferred_element_type=jnp.float32)  8.9 us
  transfers between devices with their start and end apart: 5, of which 5 were waited for; matrix products, arithmetic and copies ran while one was open for 1% of the time, Pallas kernels for 0%

commit v1 on v0

--- a/solution.py
+++ b/solution.py
@@ -43,7 +43,12 @@
     )
     state = (empty, empty)
     key_piece = lax.all_gather(key_pairs, "sp", axis=0, tiled=True)
-    value_piece = lax.all_gather(values, "sp", axis=0, tiled=True)
+    value_piece = jnp.concatenate(
+        lax.all_to_all(
+            jnp.stack(lax.axis_size("sp") * [values]), axis_name="sp", split_axis=0, concat_axis=0
+        ),
+        axis=0,
+    )
     length = key_piece.shape[0]
     span = length
     for split_count in range(1, length + 1):

time: 431 us -> 412 us (0.956)
  blocking collectives: 71.5 us -> 44.8 us
  starting transfers between devices: 0.16 us -> 7.47 us
    all_gather x1 -> x0, blocking collectives: 31.3 us -> none  [on_device(): value_piece = lax.all_gather(values, 'sp', axis=0, tiled=True)]
    all_to_all x0 -> x1, starting transfers between devices: none -> 7.28 us  [on_device(): lax.all_to_all(jnp.stack(lax.axis_size('sp') * [values]), axis_name='sp',...]
    all_gather x1, blocking collectives: 33 us -> 37.6 us  [on_device(): key_piece = lax.all_gather(key_pairs, 'sp', axis=0, tiled=True)]
  transfers between devices with their start and end apart: 5 -> 6, of which waited for: 5 -> 5; matrix products, arithmetic and copies ran while one was open for 1% -> 2% of each run, Pallas kernels for 0% -> 0%
where the time goes in v1:
time: 412 us
  waiting for transfers between devices  312 us (76%)
  blocking collectives  44.8 us (11%)
  matrix products  23.1 us (6%)
  between operations  13.4 us (3%)
  starting transfers between devices  7.47 us (2%)
  other arithmetic  5.98 us (1%)
  local copies, waits for them, and re-layouts  5.11 us (1%)
    all_gather x1, waiting for transfers between devices, on_device(): lax.all_gather(gate_weight, 'sp', axis=0, tiled=True)  94.5 us
    all_gather x1, waiting for transfers between devices, on_device(): lax.all_gather(up_weight, 'sp', axis=0, tiled=True)  92.6 us
    all_gather x1, waiting for transfers between devices, on_device(): down_whole = lax.all_gather(down_weight, 'sp', axis=1, tiled=True)  88.6 us
    all_gather x1, blocking collectives, on_device(): key_piece = lax.all_gather(key_pairs, 'sp', axis=0, tiled=True)  37.6 us
    reduce_scatter x1, waiting for transfers between devices, on_device(): lax.psum_scatter(jnp.dot(picked, down_whole, preferred_element_type=jnp.f...  23.2 us
    all_gather x1, waiting for transfers between devices, on_device(): gathered = lax.all_gather(normed_in, 'tp', axis=0, tiled=True)  11.1 us
    dot_general x1, matrix products, on_device(): jnp.dot(picked, down_whole, preferred_element_type=jnp.float32)  8.91 us
  transfers between devices with their start and end apart: 6, of which 5 were waited for; matrix products, arithmetic and copies ran while one was open for 2% of the time, Pallas kernels for 0%

profile of v1, /device:TPU:0, one launch (start us, length us, event | category | flops | bytes accessed | tf_op | source)
XLA Modules:
  0.0 411.7 jit_solution(6058459136460741702)
XLA Ops:
  6.5 0.0 copy-start
  6.5 1.8 stack.2
  8.3 7.3 %all-to-all-start = ((bf16[8,256,128]{2,1,0:T(8,128)(2,1)}), bf16[8,256,128]{2,1,0:T(8,128)(2,1)S(1)}, u32[]{:S(2)}, u32[]{:S(2)}) async-start(bf16[8,256,128]{2,1,0:T(8,128)(2,1)} %stack.2), calls=%async_computation | async-start | bytes 1048576 | tf_op jit(solution)/shard_map/all_to_all | solution.py:47
  15.6 0.0 all-gather.5.cloned.1.call-start
  15.6 0.9 copy.16
  16.6 37.6 %all_gather.15 = bf16[2048,128]{0,1:T(8,128)(2,1)S(1)} all-gather(bf16[256,128]{0,1:T(8,128)(2,1)S(1)} %copy.16), channel_id=1, replica_groups=mesh['sp'=8,'tp'=4] {'sp'}, dimensions={0}, use_global_device_ids=true | all-gather | bytes 589824 | tf_op jit(solution)/shard_map/all_gather | solution.py:45
  54.2 1.0 copy.14
  55.2 0.1 copy.15
  55.3 0.8 multiply_reduce_fusion.1
  56.1 0.0 copy-start.1
  56.2 0.1 copy.17
  56.3 0.8 multiply_reduce_fusion
  57.1 0.0 copy-done
  57.1 0.0 copy-start.2
  57.1 0.1 broadcast_bitcast_fusion
  57.2 0.8 fusion
  58.0 0.1 copy-done.1
  58.1 0.8 fusion.2
  58.9 0.5 copy-done.2
  59.4 0.0 all-to-all-done
  59.4 0.0 copy-start.3
  59.4 3.2 fusion.29
  62.6 0.0 copy-start.8
  62.7 0.2 copy-done.3
  62.9 1.4 multiply_reduce_fusion.4
  64.3 0.0 copy-start.4
  64.3 0.0 copy-start.5
  64.3 0.0 copy-start.6
  64.3 0.0 copy-done.8
  64.4 0.1 multiply_convert_fusion.1
  64.5 0.1 copy.25
  64.6 0.1 reshape_reshape.4
  64.7 7.2 %all_to_all.20 = bf16[4,64,256]{2,1,0:T(8,128)(2,1)S(1)} all-to-all(bf16[4,64,256]{2,1,0:T(8,128)(2,1)S(1)} %reshape_reshape.4), channel_id=1, replica_groups=mesh['sp'=8,'tp'=4] {'tp'}, dimensions={0} | all-to-all | bytes 262144 | tf_op jit(solution)/shard_map/all_to_all | solution.py:94
  71.9 0.1 copy.19
  72.1 3.2 multiply_reduce_fusion.3
  75.2 0.0 copy-done.4
  75.2 0.0 copy-done.5
  75.2 0.3 multiply_reduce_fusion.2
  75.5 0.0 copy-done.6
  75.5 0.9 multiply_convert_fusion
  76.4 0.0 all-gather.5.cloned.1.call-update
  76.5 0.0 all-gather.7.cloned.1.call-start
  76.5 0.7 all-gather.7.cloned.1.call-update
  77.2 0.0 all-gather.11.cloned.1.call-start
  77.2 0.7 all-gather.11.cloned.1.call-update
  77.9 0.0 all-gather.9.cloned.1.call-start
  78.0 0.5 all-gather.9.cloned.1.call-update
  78.5 0.0 reduce-scatter.2.cloned.1.call-start
  78.6 11.1 %all-gather.5.cloned.1.call-done = bf16[256,2048]{1,0:T(8,128)(2,1)} async-done(((bf16[64,2048]{1,0:T(8,128)(2,1)}), bf16[256,2048]{1,0:T(8,128)(2,1)}) %all-gather.5.cloned.1.call-update) | async-done | bytes 1048592 | tf_op jit(solution)/shard_map/all_gather | solution.py:100
  89.6 0.0 copy-start.9
  89.6 94.5 %all-gather.7.cloned.1.call-done = bf16[2048,1408]{1,0:T(8,128)(2,1)} async-done(((bf16[256,1408]{1,0:T(8,128)(2,1)}), bf16[2048,1408]{1,0:T(8,128)(2,1)}) %all-gather.7.cloned.1.call-update) | async-done | bytes 5767184 | tf_op jit(solution)/shard_map/all_gather | solution.py:103
  184.1 4.8 %fusion.45 = f32[256,1408]{1,0:T(8,128)S(1)} fusion(bf16[256,2048]{1,0:T(8,128)(2,1)} %all-gather.5.cloned.1.call-done, bf16[2048,1408]{1,0:T(8,128)(2,1)} %all-gather.7.cloned.1.call-done), kind=kOutput, calls=%fused_computation.58 | convolution fusion | flops 1476395008 | bytes 8257536 | tf_op jit(solution)/shard_map/dot_general | solution.py:107
  188.9 0.0 copy-start.7
  188.9 88.6 %all-gather.11.cloned.1.call-done = bf16[1408,2048]{1,0:T(8,128)(2,1)} async-done(((bf16[1408,256]{1,0:T(8,128)(2,1)}), bf16[1408,2048]{1,0:T(8,128)(2,1)}) %all-gather.11.cloned.1.call-update) | async-done | bytes 5767184 | tf_op jit(solution)/shard_map/all_gather | solution.py:111
  277.5 92.6 %all-gather.9.cloned.1.call-done = bf16[2048,1408]{1,0:T(8,128)(2,1)} async-done(((bf16[256,1408]{1,0:T(8,128)(2,1)}), bf16[2048,1408]{1,0:T(8,128)(2,1)}) %all-gather.9.cloned.1.call-update) | async-done | bytes 5767184 | tf_op jit(solution)/shard_map/all_gather | solution.py:104
  370.1 0.0 copy-done.9
  370.1 8.9 %convolution_convert_fusion = bf16[256,2048]{1,0:T(8,128)(2,1)} fusion(bf16[1408,2048]{1,0:T(8,128)(2,1)} %all-gather.11.cloned.1.call-done, bf16[256,2048]{1,0:T(8,128)(2,1)S(1)} %copy-done.9, bf16[2048,1408]{1,0:T(8,128)(2,1)} %all-gather.9.cloned.1.call-done, f32[256,1408]{1,0:T(8,128)S(1)} %fusion.45), kind=kOutput, calls=%fused_computation.10 | convolution fusion | flops 2955476992 | bytes 15073280 | tf_op jit(solution)/shard_map/dot_general | solution.py:115
  379.0 0.0 reduce-scatter.2.cloned.1.call-update
  379.0 23.2 %reduce-scatter.2.cloned.1.call-done = bf16[64,2048]{1,0:T(8,128)(2,1)} async-done(((bf16[256,2048]{1,0:T(8,128)(2,1)}), bf16[64,2048]{1,0:T(8,128)(2,1)}) %reduce-scatter.2.cloned.1.call-update) | async-done | bytes 262160 | tf_op jit(solution)/shard_map/reduce_scatter | solution.py:114
  402.2 1.1 fusion.32
  403.3 0.0 copy-done.7
  403.3 1.9 fusion.36
  (13 shorter events, 0.1 us)
Async XLA Ops:
  6.5 50.5 %copy-start = (f32[2]{0:T(128)S(1)}, f32[2]{0:T(128)}, u32[]{:S(2)}) copy-start(f32[2]{0:T(128)} %param.17) | copy-start | bytes 28
  8.3 51.1 %all-to-all-start = ((bf16[8,256,128]{2,1,0:T(8,128)(2,1)}), bf16[8,256,128]{2,1,0:T(8,128)(2,1)S(1)}, u32[]{:S(2)}, u32[]{:S(2)}) async-start(bf16[8,256,128]{2,1,0:T(8,128)(2,1)} %stack.2), calls=%async_computation | async-start | bytes 1048576 | tf_op jit(solution)/shard_map/all_to_all | solution.py:47
  15.6 74.1 %all-gather.5.cloned.1.call-start = ((), (), s32[]{:S(2)}) async-start(), calls=%async_computation.3 | async-start | bytes 1310720 | tf_op jit(solution)/shard_map/all_gather | solution.py:100
  56.1 1.9 copy-start.1
  57.1 2.3 copy-start.2
  59.4 3.5 copy-start.3
  62.6 1.7 copy-start.8
  64.3 10.9 %copy-start.4 = (bf16[64,2048]{1,0:T(8,128)(2,1)S(1)}, bf16[64,2048]{1,0:T(8,128)(2,1)}, u32[]{:S(2)}) copy-start(bf16[64,2048]{1,0:T(8,128)(2,1)} %param.13) | copy-start | bytes 786436
  64.3 10.9 %copy-start.5 = (f32[2048]{0:T(1024)S(1)}, f32[2048]{0:T(1024)}, u32[]{:S(2)}) copy-start(f32[2048]{0:T(1024)} %param.20) | copy-start | bytes 24580
  64.3 11.2 %copy-start.6 = (f32[2048]{0:T(1024)S(1)}, f32[2048]{0:T(1024)}, u32[]{:S(2)}) copy-start(f32[2048]{0:T(1024)} %param.21) | copy-start | bytes 24580
  76.5 107.7 %all-gather.7.cloned.1.call-start = ((), (), s32[]{:S(2)}) async-start(), calls=%async_computation.4 | async-start | bytes 6488064 | tf_op jit(solution)/shard_map/all_gather | solution.py:103
  77.2 200.3 %all-gather.11.cloned.1.call-start = ((), (), s32[]{:S(2)}) async-start(), calls=%async_computation.6 | async-start | bytes 6488064 | tf_op jit(solution)/shard_map/all_gather | solution.py:111
  77.9 292.2 %all-gather.9.cloned.1.call-start = ((), (), s32[]{:S(2)}) async-start(), calls=%async_computation.5 | async-start | bytes 6488064 | tf_op jit(solution)/shard_map/all_gather | solution.py:104
  78.5 323.7 %reduce-scatter.2.cloned.1.call-start = ((), (), s32[]{:S(2)}) async-start(), calls=%async_computation.7 | async-start | bytes 1310720 | tf_op jit(solution)/shard_map/reduce_scatter | solution.py:114
  89.6 280.5 %copy-start.9 = (bf16[256,2048]{1,0:T(8,128)(2,1)S(1)}, bf16[256,2048]{1,0:T(8,128)(2,1)}, u32[]{:S(2)}) copy-start(bf16[256,2048]{1,0:T(8,128)(2,1)} %all-gather.5.cloned.1.call-done) | copy-start | bytes 3145732
  188.9 214.4 %copy-start.7 = (f32[2048]{0:T(1024)S(1)}, f32[2048]{0:T(1024)}, u32[]{:S(2)}) copy-start(f32[2048]{0:T(1024)} %param.22) | copy-start | bytes 24580
Sparse Core Ops, SparseCore 0:
  76.6 13.0 all-gather.4
  91.8 92.2 all-gather.6
  186.2 91.2 all-gather.10
  279.6 90.4 all-gather.8
  379.2 22.9 reduce-scatter.1
